TPU v7x, 32 devices: a whole 2x2x4 slice. The times are simulated.
32 devices in a mesh: grp: 2 (over y), sp: 4 (over z), tp: 4 (over x, core).
Axes of the slice: x: 2, y: 2, z: 4, core: 2. Of those that a mesh axis runs over, the one named last changes fastest.
Arguments:
- tokens_in: bfloat16 [2048, 2048], P(('grp', 'sp'), 'tp'), parts along dimension 0, may hold values from -6 to 6
- norm_gain: float32 [3, 2048], replicated, may hold values from 0.1 to 1.9
- w_pool_in: bfloat16 [3, 2048, 1024], P(None, 'sp', 'tp'), may hold values from -0.125 to 0.125
- w_gate: bfloat16 [3, 2048, 2048], P(None, 'sp', 'tp'), may hold values from -0.125 to 0.125
- w_back: bfloat16 [3, 1024, 2048], P(None, 'tp', 'sp'), may hold values from -0.25 to 0.25
Outputs:
- tokens_out: bfloat16 [2048, 2048], P(('grp', 'sp'), 'tp'), parts along dimension 0
There are 2 independent parts, one for each index of `grp`. A program takes and returns all parts, laid end to end along the dimension named above; an argument that names none is the same for every part. Nothing has to cross between parts.
All inputs are finite; a program needn't handle non-finite values.
Results may differ from a plain program's by a relative error of at most 0.017.
Values may be sent and summed in bfloat16 or wider, within the bound.
A program may use at most 64 MiB of HBM per device.

v0:
```python
import jax
import jax.numpy as jnp
from jax import lax
from jax.sharding import PartitionSpec as P

POOL_WIDTH = 1024
GROUPS = 4
GRID_W = 32
LAYERS = 3
pool_windows = (2, 4, 8, 16)
norm_eps = 1e-06


def padded_2(value, sides, width):
    for axis, dim in sides:
        peers, length = (lax.axis_size(axis), value.shape[dim])
        up = [(i, (i + 1) % peers) for i in range(peers - 1)]
        down = [(j, i) for i, j in up]
        last = lax.slice_in_dim(value, length - width, length, axis=dim)
        initial = lax.slice_in_dim(value, 0, width, axis=dim)
        before = lax.ppermute(last, axis, up)
        after = lax.ppermute(initial, axis, down)
        value = jnp.concatenate([before, value, after], axis=dim)
    return value


def window_means(padded, rows_here, first_row, total_rows, window):
    reach = max(pool_windows) // 2
    half_span = window // 2
    width_cols = padded.shape[1] - 2 * reach
    row_sums = padded[reach - half_span : reach - half_span + rows_here]
    for offset in range(1 - half_span, half_span):
        row_sums = row_sums + padded[reach + offset : reach + offset + rows_here]
    box_sums = row_sums[:, reach - half_span : reach - half_span + width_cols]
    for offset in range(1 - half_span, half_span):
        box_sums = box_sums + row_sums[:, reach + offset : reach + offset + width_cols]
    row_index = first_row + jnp.arange(rows_here, dtype=jnp.int32)
    col_index = jnp.arange(width_cols, dtype=jnp.int32)
    row_counts = jnp.minimum(row_index + half_span, total_rows) - jnp.maximum(
        row_index - half_span, 0
    )
    col_counts = jnp.minimum(col_index + half_span, width_cols) - jnp.maximum(
        col_index - half_span, 0
    )
    counts = (row_counts[:, None] * col_counts[None, :]).astype(jnp.float32)
    return box_sums / counts[:, :, None]


def on_device(tokens_in, norm_gain, w_pool_in, w_gate, w_back):
    reach = max(pool_windows) // 2
    sp_count = lax.axis_size("sp")
    tp_count = lax.axis_size("tp")
    tp_pos = lax.axis_index("tp")
    sp_pos = lax.axis_index("sp")
    tok_rows = tokens_in.shape[0]
    rows_here = tok_rows // GRID_W
    total_rows = rows_here * sp_count
    first_row = sp_pos * rows_here
    local_pool = w_pool_in.shape[2]
    group_width = POOL_WIDTH // GROUPS
    channel_group = (tp_pos * local_pool + jnp.arange(local_pool, dtype=jnp.int32)) // group_width
    state = tokens_in
    for layer_id in range(LAYERS):
        whole_rows = lax.all_gather(state, "tp", axis=1, tiled=True)
        wide = whole_rows.astype(jnp.float32)
        normed = (
            wide
            * lax.rsqrt(jnp.mean(wide * wide, axis=-1, keepdims=True) + norm_eps)
            * norm_gain[layer_id]
        ).astype(jnp.bfloat16)
        pool_acc = jnp.dot(
            normed,
            lax.all_gather(w_pool_in[layer_id], "sp", axis=0, tiled=True),
            preferred_element_type=jnp.float32,
        )
        gate_acc = jnp.dot(
            normed,
            lax.all_gather(w_gate[layer_id], "sp", axis=0, tiled=True),
            preferred_element_type=jnp.float32,
        )
        pool_in = pool_acc.astype(jnp.bfloat16)
        gate = jax.nn.sigmoid(gate_acc)
        cells = pool_in.reshape(rows_here, GRID_W, local_pool)
        rimmed = padded_2(cells, (("sp", 0),), reach)
        padded = jnp.pad(rimmed.astype(jnp.float32), ((0, 0), (reach, reach), (0, 0)))
        means = jnp.zeros((rows_here, GRID_W, local_pool), jnp.float32)
        for group_id in range(GROUPS):
            in_group = (channel_group == group_id)[None, None, :]
            means = jnp.where(
                in_group,
                window_means(padded, rows_here, first_row, total_rows, pool_windows[group_id]),
                means,
            )
        pooled = (
            (means - cells.astype(jnp.float32)).reshape(tok_rows, local_pool).astype(jnp.bfloat16)
        )
        full_pooled = lax.all_gather(pooled, "tp", axis=1, tiled=True)
        back_rows = lax.all_gather(w_back[layer_id], "sp", axis=1, tiled=True)
        back_cols = lax.all_to_all(back_rows, "tp", split_axis=1, concat_axis=0, tiled=True)
        partials = jnp.einsum(
            "tnb,nbd->ntd",
            full_pooled.reshape(tok_rows, tp_count, local_pool),
            back_cols.reshape(tp_count, local_pool, back_cols.shape[1]),
            preferred_element_type=jnp.float32,
        ).astype(jnp.bfloat16)
        branch = jnp.sum(partials.astype(jnp.float32), axis=0)
        state = (state.astype(jnp.float32) + gate * branch).astype(jnp.bfloat16)
    return state


def solution(mesh):
    return jax.shard_map(
        on_device,
        mesh=mesh,
        in_specs=(
            P(("grp", "sp"), "tp"),
            P(),
            P(None, "sp", "tp"),
            P(None, "sp", "tp"),
            P(None, "tp", "sp"),
        ),
        out_specs=P(("grp", "sp"), "tp"),
        check_vma=False,
    )
```

profile of v0, /device:TPU:0, one launch (start us, length us, event | category | flops | bytes accessed | tf_op | source)
XLA Modules:
  0.0 391.0 jit_solution(7945444731493379469)
XLA Ops:
  6.5 0.7 all-gather.22.cloned.1.call-update
  7.3 2.2 fusion.168
  9.6 0.8 fusion.167
  10.3 0.8 copy.33
  11.3 1.2 fusion.166
  12.9 0.6 fusion.169
  13.5 14.9 %all-gather.22.cloned.1.call-done = bf16[256,2048]{1,0:T(8,128)(2,1)} async-done(((bf16[256,512]{1,0:T(8,128)(2,1)}), bf16[256,2048]{1,0:T(8,128)(2,1)}) %all-gather.22.cloned.1.call-update) | async-done | bytes 1048592 | tf_op jit(solution)/shard_map/all_gather | solution.py:64
  28.3 1.5 fusion
  29.9 28.1 %all-gather.30.cloned.1.call-done = bf16[1,2048,256]{2,1,0:T(8,128)(2,1)} async-done(((bf16[1,512,256]{2,1,0:T(8,128)(2,1)}), bf16[1,2048,256]{2,1,0:T(8,128)(2,1)}) %all-gather.30.cloned.1.call-update) | async-done | bytes 1048592 | tf_op jit(solution)/shard_map/all_gather | solution.py:73
  57.9 2.0 convolution_convert_fusion.5
  60.0 3.4 collective-permute-start
  63.3 1.3 collective-permute-start.1
  64.7 23.0 %all-gather.32.cloned.1.call-done = bf16[1,256,2048]{1,2,0:T(8,128)(2,1)} async-done(((bf16[1,256,512]{1,2,0:T(8,128)(2,1)}), bf16[1,256,2048]{1,2,0:T(8,128)(2,1)}) %all-gather.32.cloned.1.call-update) | async-done | bytes 1048592 | tf_op jit(solution)/shard_map/all_gather | solution.py:98
  87.7 2.3 copy.20
  90.0 3.5 all-to-all-start
  94.1 0.8 fusion.151
  94.9 16.6 %all_gather.48 = bf16[256,1024]{1,0:T(8,128)(2,1)S(1)} all-gather(bf16[256,256]{1,0:T(8,128)(2,1)S(1)} %bitcast.112), channel_id=1, replica_groups=mesh['grp'=2,'sp'=4,'tp'=4] {'tp'}, dimensions={1}, use_global_device_ids=true | all-gather | bytes 655360 | tf_op jit(solution)/shard_map/all_gather | solution.py:97
  112.3 21.1 %all-gather.28.cloned.1.call-done = bf16[1,2048,512]{2,1,0:T(8,128)(2,1)} async-done(((bf16[1,512,512]{2,1,0:T(8,128)(2,1)}), bf16[1,2048,512]{2,1,0:T(8,128)(2,1)}) %all-gather.28.cloned.1.call-update) | async-done | bytes 2097168 | tf_op jit(solution)/shard_map/all_gather | solution.py:78
  133.4 3.2 fusion.75
  137.2 0.8 copy.34
  138.1 0.7 all-gather.34.cloned.1.call-update
  138.8 13.4 %all-gather.24.cloned.1.call-done = bf16[256,2048]{1,0:T(8,128)(2,1)} async-done(((bf16[256,512]{1,0:T(8,128)(2,1)}), bf16[256,2048]{1,0:T(8,128)(2,1)}) %all-gather.24.cloned.1.call-update) | async-done | bytes 1048592 | tf_op jit(solution)/shard_map/all_gather | solution.py:64
  152.2 1.5 fusion.3
  153.8 27.9 %all-gather.36.cloned.1.call-done = bf16[1,2048,256]{2,1,0:T(8,128)(2,1)} async-done(((bf16[1,512,256]{2,1,0:T(8,128)(2,1)}), bf16[1,2048,256]{2,1,0:T(8,128)(2,1)}) %all-gather.36.cloned.1.call-update) | async-done | bytes 1048592 | tf_op jit(solution)/shard_map/all_gather | solution.py:73
  181.7 2.0 convolution_convert_fusion.4
  183.7 3.4 collective-permute-start.2
  187.1 1.3 collective-permute-start.3
  188.4 23.1 %all-gather.38.cloned.1.call-done = bf16[1,256,2048]{1,2,0:T(8,128)(2,1)} async-done(((bf16[1,256,512]{1,2,0:T(8,128)(2,1)}), bf16[1,256,2048]{1,2,0:T(8,128)(2,1)}) %all-gather.38.cloned.1.call-update) | async-done | bytes 1048592 | tf_op jit(solution)/shard_map/all_gather | solution.py:98
  211.5 2.3 copy.24
  213.7 3.5 all-to-all-start.1
  218.4 0.8 fusion.152
  219.2 16.1 %all_gather.53 = bf16[256,1024]{1,0:T(8,128)(2,1)S(1)} all-gather(bf16[256,256]{1,0:T(8,128)(2,1)S(1)} %bitcast.113), channel_id=1, replica_groups=mesh['grp'=2,'sp'=4,'tp'=4] {'tp'}, dimensions={1}, use_global_device_ids=true | all-gather | bytes 655360 | tf_op jit(solution)/shard_map/all_gather | solution.py:97
  236.0 21.2 %all-gather.34.cloned.1.call-done = bf16[1,2048,512]{2,1,0:T(8,128)(2,1)} async-done(((bf16[1,512,512]{2,1,0:T(8,128)(2,1)}), bf16[1,2048,512]{2,1,0:T(8,128)(2,1)}) %all-gather.34.cloned.1.call-update) | async-done | bytes 2097168 | tf_op jit(solution)/shard_map/all_gather | solution.py:78
  257.3 3.1 fusion.72
  261.1 0.8 copy.35
  262.5 13.6 %all-gather.26.cloned.1.call-done = bf16[256,2048]{1,0:T(8,128)(2,1)} async-done(((bf16[256,512]{1,0:T(8,128)(2,1)}), bf16[256,2048]{1,0:T(8,128)(2,1)}) %all-gather.26.cloned.1.call-update) | async-done | bytes 1048592 | tf_op jit(solution)/shard_map/all_gather | solution.py:64
  276.1 1.5 fusion.6
  277.6 27.9 %all-gather.42.cloned.1.call-done = bf16[1,2048,256]{2,1,0:T(8,128)(2,1)} async-done(((bf16[1,512,256]{2,1,0:T(8,128)(2,1)}), bf16[1,2048,256]{2,1,0:T(8,128)(2,1)}) %all-gather.42.cloned.1.call-update) | async-done | bytes 1048592 | tf_op jit(solution)/shard_map/all_gather | solution.py:73
  305.5 2.0 convolution_convert_fusion.3
  307.6 3.4 collective-permute-start.4
  310.9 1.3 collective-permute-start.5
  312.2 23.1 %all-gather.44.cloned.1.call-done = bf16[1,256,2048]{1,2,0:T(8,128)(2,1)} async-done(((bf16[1,256,512]{1,2,0:T(8,128)(2,1)}), bf16[1,256,2048]{1,2,0:T(8,128)(2,1)}) %all-gather.44.cloned.1.call-update) | async-done | bytes 1048592 | tf_op jit(solution)/shard_map/all_gather | solution.py:98
  335.3 2.3 copy.28
  337.6 3.7 all-to-all-start.2
  342.3 0.8 fusion.153
  343.1 16.1 %all_gather.58 = bf16[256,1024]{1,0:T(8,128)(2,1)S(1)} all-gather(bf16[256,256]{1,0:T(8,128)(2,1)S(1)} %bitcast.111), channel_id=1, replica_groups=mesh['grp'=2,'sp'=4,'tp'=4] {'tp'}, dimensions={1}, use_global_device_ids=true | all-gather | bytes 655360 | tf_op jit(solution)/shard_map/all_gather | solution.py:97
  359.9 21.1 %all-gather.40.cloned.1.call-done = bf16[1,2048,512]{2,1,0:T(8,128)(2,1)} async-done(((bf16[1,512,512]{2,1,0:T(8,128)(2,1)}), bf16[1,2048,512]{2,1,0:T(8,128)(2,1)}) %all-gather.40.cloned.1.call-update) | async-done | bytes 2097168 | tf_op jit(solution)/shard_map/all_gather | solution.py:78
  381.0 3.1 fusion.69
  (113 shorter events, 7.0 us)
Async XLA Ops:
  6.5 3.0 copy-start.5
  6.5 21.8 %all-gather.22.cloned.1.call-start = ((), (), s32[]{:S(2)}) async-start(), calls=%async_computation.3 | async-start | bytes 1310720 | tf_op jit(solution)/shard_map/all_gather | solution.py:64
  7.3 4.0 %copy-start = (bf16[3,512,512]{2,1,0:T(8,128)(2,1)S(1)}, bf16[3,512,512]{2,1,0:T(8,128)(2,1)}, u32[]{:S(2)}) copy-start(bf16[3,512,512]{2,1,0:T(8,128)(2,1)} %param.8) | copy-start | bytes 4718596
  7.3 50.7 %all-gather.30.cloned.1.call-start = ((), (), s32[]{:S(2)}) async-start(), calls=%async_computation.7 | async-start | bytes 1310720 | tf_op jit(solution)/shard_map/all_gather | solution.py:73
  9.5 78.2 %all-gather.32.cloned.1.call-start = ((), (), s32[]{:S(2)}) async-start(), calls=%async_computation.8 | async-start | bytes 1310720 | tf_op jit(solution)/shard_map/all_gather | solution.py:98
  11.2 1.7 copy-start.6
  11.2 122.2 %all-gather.28.cloned.1.call-start = ((), (), s32[]{:S(2)}) async-start(), calls=%async_computation.6 | async-start | bytes 2621440 | tf_op jit(solution)/shard_map/all_gather | solution.py:78
  13.5 46.5 %copy-start.10 = (f32[1,2048]{1,0:T(1,128)}, f32[1,2048]{1,0:T(1,128)S(1)}, u32[]{:S(2)}) copy-start(f32[1,2048]{1,0:T(1,128)S(1)} %get-tuple-element.27) | copy-start | bytes 24580
  29.9 60.1 %copy-start.23 = (f32[256]{0:T(256)}, f32[256]{0:T(256)S(1)}, u32[]{:S(2)}) copy-start(f32[256]{0:T(256)S(1)} %add_rsqrt_fusion.2) | copy-start | bytes 3076
  60.0 33.6 %collective-permute-start = (bf16[8,32,256]{2,1,0:T(8,128)(2,1)S(1)}, bf16[8,32,256]{2,1,0:T(8,128)(2,1)S(1)}, u32[]{:S(2)}, u32[]{:S(2)}) collective-permute-start(bf16[8,32,256]{2,1,0:T(8,128)(2,1)S(1)} %bitcast.99), channel_id=1, source_target_pairs={{0,4},{4,8},{8,12},{1,5},{5,9},{9,13},{2,6},{6,10},{10,14},{3,7},{... | collective-permute-start | bytes 393224 | tf_op jit(solution)/shard_map/ppermute | solution.py:21
  63.3 30.2 %collective-permute-start.1 = (bf16[8,32,256]{2,1,0:T(8,128)(2,1)S(1)}, bf16[8,32,256]{2,1,0:T(8,128)(2,1)S(1)}, u32[]{:S(2)}, u32[]{:S(2)}) collective-permute-start(bf16[8,32,256]{2,1,0:T(8,128)(2,1)S(1)} %bitcast.100), channel_id=1, source_target_pairs={{4,0},{8,4},{12,8},{5,1},{9,5},{13,9},{6,2},{10,6},{14,10},{7,3},{... | collective-permute-start | bytes 393224 | tf_op jit(solution)/shard_map/ppermute | solution.py:22
  64.7 29.4 %copy-start.11 = (pred[256]{0:T(512)(128)(4,1)}, pred[256]{0:T(512)(128)(4,1)S(1)}, u32[]{:S(2)}) copy-start(pred[256]{0:T(512)(128)(4,1)S(1)} %get-tuple-element.33) | copy-start | bytes 772
  64.7 29.4 %copy-start.14 = (pred[256]{0:T(512)(128)(4,1)}, pred[256]{0:T(512)(128)(4,1)S(1)}, u32[]{:S(2)}) copy-start(pred[256]{0:T(512)(128)(4,1)S(1)} %get-tuple-element.34) | copy-start | bytes 772
  64.7 29.4 %copy-start.17 = (pred[256]{0:T(512)(128)(4,1)}, pred[256]{0:T(512)(128)(4,1)S(1)}, u32[]{:S(2)}) copy-start(pred[256]{0:T(512)(128)(4,1)S(1)} %get-tuple-element.35) | copy-start | bytes 772
  64.7 29.4 %copy-start.20 = (pred[256]{0:T(512)(128)(4,1)}, pred[256]{0:T(512)(128)(4,1)S(1)}, u32[]{:S(2)}) copy-start(pred[256]{0:T(512)(128)(4,1)S(1)} %get-tuple-element.36) | copy-start | bytes 772
  90.0 21.8 %all-to-all-start = ((bf16[256,4,512]{2,0,1:T(8,128)(2,1)}), bf16[256,4,512]{2,0,1:T(8,128)(2,1)S(1)}, u32[]{:S(2)}, u32[]{:S(2)}) async-start(bf16[256,4,512]{2,0,1:T(8,128)(2,1)} %copy.20), calls=%async_computation | async-start | bytes 2097152 | tf_op jit(solution)/shard_map/all_to_all | solution.py:99
  93.5 58.7 %all-gather.24.cloned.1.call-start = ((), (), s32[]{:S(2)}) async-start(), calls=%async_computation.4 | async-start | bytes 1310720 | tf_op jit(solution)/shard_map/all_gather | solution.py:64
  94.9 38.5 %copy-start.1 = (bf16[256,2048]{1,0:T(8,128)(2,1)S(1)}, bf16[256,2048]{1,0:T(8,128)(2,1)}, u32[]{:S(2)}) copy-start(bf16[256,2048]{1,0:T(8,128)(2,1)} %all-gather.22.cloned.1.call-done) | copy-start | bytes 3145732
  112.3 24.9 %copy-start.4 = (bf16[1,256,512]{2,1,0:T(8,128)(2,1)S(1)}, bf16[1,256,512]{2,1,0:T(8,128)(2,1)}, u32[]{:S(2)}) copy-start(bf16[1,256,512]{2,1,0:T(8,128)(2,1)} %get-tuple-element.21) | copy-start | bytes 786436
  136.5 45.1 %copy-start.8 = (f32[1,2048]{1,0:T(1,128)S(1)}, f32[1,2048]{1,0:T(1,128)}, u32[]{:S(2)}) copy-start(f32[1,2048]{1,0:T(1,128)} %get-tuple-element.28) | copy-start | bytes 24580
  136.6 45.1 %all-gather.36.cloned.1.call-start = ((), (), s32[]{:S(2)}) async-start(), calls=%async_computation.10 | async-start | bytes 1310720 | tf_op jit(solution)/shard_map/all_gather | solution.py:73
  137.1 74.3 %all-gather.38.cloned.1.call-start = ((), (), s32[]{:S(2)}) async-start(), calls=%async_computation.11 | async-start | bytes 1310720 | tf_op jit(solution)/shard_map/all_gather | solution.py:98
  138.1 119.2 %all-gather.34.cloned.1.call-start = ((), (), s32[]{:S(2)}) async-start(), calls=%async_computation.9 | async-start | bytes 2621440 | tf_op jit(solution)/shard_map/all_gather | solution.py:78
  153.8 60.0 %copy-start.24 = (f32[256]{0:T(256)}, f32[256]{0:T(256)S(1)}, u32[]{:S(2)}) copy-start(f32[256]{0:T(256)S(1)} %add_rsqrt_fusion.1) | copy-start | bytes 3076
  183.7 33.6 %collective-permute-start.2 = (bf16[8,32,256]{2,1,0:T(8,128)(2,1)S(1)}, bf16[8,32,256]{2,1,0:T(8,128)(2,1)S(1)}, u32[]{:S(2)}, u32[]{:S(2)}) collective-permute-start(bf16[8,32,256]{2,1,0:T(8,128)(2,1)S(1)} %bitcast.107), channel_id=1, source_target_pairs={{0,4},{4,8},{8,12},{1,5},{5,9},{9,13},{2,6},{6,10},{10,14},{3,7},{... | collective-permute-start | bytes 393224 | tf_op jit(solution)/shard_map/ppermute | solution.py:21
  187.1 30.3 %collective-permute-start.3 = (bf16[8,32,256]{2,1,0:T(8,128)(2,1)S(1)}, bf16[8,32,256]{2,1,0:T(8,128)(2,1)S(1)}, u32[]{:S(2)}, u32[]{:S(2)}) collective-permute-start(bf16[8,32,256]{2,1,0:T(8,128)(2,1)S(1)} %bitcast.108), channel_id=1, source_target_pairs={{4,0},{8,4},{12,8},{5,1},{9,5},{13,9},{6,2},{10,6},{14,10},{7,3},{... | collective-permute-start | bytes 393224 | tf_op jit(solution)/shard_map/ppermute | solution.py:22
  213.7 21.8 %all-to-all-start.1 = ((bf16[256,4,512]{2,0,1:T(8,128)(2,1)}), bf16[256,4,512]{2,0,1:T(8,128)(2,1)S(1)}, u32[]{:S(2)}, u32[]{:S(2)}) async-start(bf16[256,4,512]{2,0,1:T(8,128)(2,1)} %copy.24), calls=%async_computation.1 | async-start | bytes 2097152 | tf_op jit(solution)/shard_map/all_to_all | solution.py:99
  217.3 58.8 %all-gather.26.cloned.1.call-start = ((), (), s32[]{:S(2)}) async-start(), calls=%async_computation.5 | async-start | bytes 1310720 | tf_op jit(solution)/shard_map/all_gather | solution.py:64
  217.7 0.6 copy-start.12
  217.7 0.6 copy-start.15
  217.7 0.7 copy-start.18
  217.7 0.7 copy-start.21
  219.2 38.1 %copy-start.3 = (bf16[256,2048]{1,0:T(8,128)(2,1)S(1)}, bf16[256,2048]{1,0:T(8,128)(2,1)}, u32[]{:S(2)}) copy-start(bf16[256,2048]{1,0:T(8,128)(2,1)} %all-gather.24.cloned.1.call-done) | copy-start | bytes 3145732
  219.2 38.0 %copy-start.9 = (f32[1,2048]{1,0:T(1,128)S(1)}, f32[1,2048]{1,0:T(1,128)}, u32[]{:S(2)}) copy-start(f32[1,2048]{1,0:T(1,128)} %get-tuple-element.28) | copy-start | bytes 24580
  219.2 38.0 %copy-start.25 = (f32[256]{0:T(256)S(1)}, f32[256]{0:T(256)}, u32[]{:S(2)}) copy-start(f32[256]{0:T(256)} %copy-done.24) | copy-start | bytes 3076
  260.4 45.1 %copy-start.7 = (f32[1,2048]{1,0:T(1,128)S(1)}, f32[1,2048]{1,0:T(1,128)}, u32[]{:S(2)}) copy-start(f32[1,2048]{1,0:T(1,128)} %get-tuple-element.26) | copy-start | bytes 24580
  260.4 45.1 %all-gather.42.cloned.1.call-start = ((), (), s32[]{:S(2)}) async-start(), calls=%async_computation.13 | async-start | bytes 1310720 | tf_op jit(solution)/shard_map/all_gather | solution.py:73
  261.0 74.3 %all-gather.44.cloned.1.call-start = ((), (), s32[]{:S(2)}) async-start(), calls=%async_computation.14 | async-start | bytes 1310720 | tf_op jit(solution)/shard_map/all_gather | solution.py:98
  261.9 119.0 %all-gather.40.cloned.1.call-start = ((), (), s32[]{:S(2)}) async-start(), calls=%async_computation.12 | async-start | bytes 2621440 | tf_op jit(solution)/shard_map/all_gather | solution.py:78
  307.6 33.7 %collective-permute-start.4 = (bf16[8,32,256]{2,1,0:T(8,128)(2,1)S(1)}, bf16[8,32,256]{2,1,0:T(8,128)(2,1)S(1)}, u32[]{:S(2)}, u32[]{:S(2)}) collective-permute-start(bf16[8,32,256]{2,1,0:T(8,128)(2,1)S(1)} %bitcast.103), channel_id=1, source_target_pairs={{0,4},{4,8},{8,12},{1,5},{5,9},{9,13},{2,6},{6,10},{10,14},{3,7},{... | collective-permute-start | bytes 393224 | tf_op jit(solution)/shard_map/ppermute | solution.py:21
  310.9 30.4 %collective-permute-start.5 = (bf16[8,32,256]{2,1,0:T(8,128)(2,1)S(1)}, bf16[8,32,256]{2,1,0:T(8,128)(2,1)S(1)}, u32[]{:S(2)}, u32[]{:S(2)}) collective-permute-start(bf16[8,32,256]{2,1,0:T(8,128)(2,1)S(1)} %bitcast.104), channel_id=1, source_target_pairs={{4,0},{8,4},{12,8},{5,1},{9,5},{13,9},{6,2},{10,6},{14,10},{7,3},{... | collective-permute-start | bytes 393224 | tf_op jit(solution)/shard_map/ppermute | solution.py:22
  337.6 21.8 %all-to-all-start.2 = ((bf16[256,4,512]{2,0,1:T(8,128)(2,1)}), bf16[256,4,512]{2,0,1:T(8,128)(2,1)S(1)}, u32[]{:S(2)}, u32[]{:S(2)}) async-start(bf16[256,4,512]{2,0,1:T(8,128)(2,1)} %copy.28), calls=%async_computation.2 | async-start | bytes 2097152 | tf_op jit(solution)/shard_map/all_to_all | solution.py:99
  341.6 0.6 copy-start.13
  341.6 0.6 copy-start.16
  341.6 0.7 copy-start.19
  341.6 0.7 copy-start.22
  343.1 37.9 %copy-start.2 = (bf16[256,2048]{1,0:T(8,128)(2,1)S(1)}, bf16[256,2048]{1,0:T(8,128)(2,1)}, u32[]{:S(2)}) copy-start(bf16[256,2048]{1,0:T(8,128)(2,1)} %all-gather.26.cloned.1.call-done) | copy-start | bytes 3145732
Sparse Core Ops, SparseCore 0:
  8.9 19.4 all-gather.21
  29.9 27.9 all-gather.29
  59.5 28.1 all-gather.31
  89.1 44.1 all-gather.27
  136.7 15.4 all-gather.23
  153.7 27.9 all-gather.35
  183.2 28.1 all-gather.37
  213.0 44.1 all-gather.33
  260.6 15.4 all-gather.25
  277.5 27.9 all-gather.41
  307.1 28.1 all-gather.43
  336.7 44.2 all-gather.39
where the time goes:
time: 392 us; the launch traced here: 391 us
  waiting for transfers between devices  261 us (67%)
  blocking collectives  48.8 us (12%)
  starting transfers between devices  25.1 us (6%)
  matrix products  16.9 us (4%)
  local copies, waits for them, and re-layouts  15.8 us (4%)
  between operations  14.2 us (4%)
  other arithmetic  8.76 us (2%)
    all_gather x3, waiting for transfers between devices, on_device(): lax.all_gather(w_pool_in[layer_id], 'sp', axis=0, tiled=True)  83.9 us
    all_gather x3, waiting for transfers between devices, on_device(): back_rows = lax.all_gather(w_back[layer_id], 'sp', axis=1, tiled=True)  69.2 us
    all_gather x3, waiting for transfers between devices, on_device(): lax.all_gather(w_gate[layer_id], 'sp', axis=0, tiled=True)  63.4 us
    all_gather x3, blocking collectives, on_device(): full_pooled = lax.all_gather(pooled, 'tp', axis=1, tiled=True)  48.8 us
    all_gather x3, waiting for transfers between devices, on_device(): whole_rows = lax.all_gather(state, 'tp', axis=1, tiled=True)  41.8 us
    all_to_all x3, starting transfers between devices, on_device(): lax.all_to_all(back_rows, 'tp', split_axis=1, concat_axis=0, tiled=True)  10.7 us
    ppermute x3, starting transfers between devices, padded_2(): before = lax.ppermute(last, axis, up)  10.1 us
    dot_general x3, matrix products, on_device(): jnp.dot(normed, lax.all_gather(w_gate[layer_id], 'sp', axis=0, tiled=True...  9.41 us
  transfers between devices with their start and end apart: 21, of which 12 were waited for; matrix products, arithmetic and copies ran while one was open for 8% of the time, Pallas kernels for 0%

commit v1 on v0

--- a/solution.py
+++ b/solution.py
@@ -61,7 +61,14 @@
     channel_group = (tp_pos * local_pool + jnp.arange(local_pool, dtype=jnp.int32)) // group_width
     state = tokens_in
     for layer_id in range(LAYERS):
-        whole_rows = lax.all_gather(state, "tp", axis=1, tiled=True)
+        ring = [state]
+        for hop in range(3):
+            ring.append(lax.ppermute(ring[-1], "tp", [(dev, (dev + 1) % 4) for dev in range(4)]))
+        whole_rows = jnp.roll(
+            jnp.concatenate(ring[::-1], axis=1),
+            (lax.axis_index("tp") + 1) * ring[0].shape[1],
+            axis=1,
+        )
         wide = whole_rows.astype(jnp.float32)
         normed = (
             wide

time: 392 us -> 333 us (0.85)
  waiting for transfers between devices: 261 us -> 202 us
  other arithmetic: 8.76 us -> 12.8 us
    all_gather x3, waiting for transfers between devices: 83.9 us -> 17.2 us  [on_device(): lax.all_gather(w_pool_in[layer_id], 'sp', axis=0, tiled=True)]
    ppermute x0 -> x9, waiting for transfers between devices: none -> 51.2 us  [on_device(): lax.ppermute(ring[-1], 'tp', [(dev, (dev + 1) % 4) for dev in range(4)])]
    all_gather x3 -> x0, waiting for transfers between devices: 41.8 us -> none  [on_device(): whole_rows = lax.all_gather(state, 'tp', axis=1, tiled=True)]
    reduce_sum x3, other arithmetic: 4.53 us -> 8.56 us  [on_device(): jnp.mean(wide * wide, axis=-1, keepdims=True) + norm_eps]
  transfers between devices with their start and end apart: 21 -> 27, of which waited for: 12 -> 18; matrix products, arithmetic and copies ran while one was open for 8% -> 11% of each run, Pallas kernels for 0% -> 0%
where the time goes in v1:
time: 333 us; the launch traced here: 332 us
  waiting for transfers between devices  202 us (61%)
  blocking collectives  48.7 us (15%)
  starting transfers between devices  25.7 us (8%)
  local copies, waits for them, and re-layouts  15.1 us (5%)
  matrix products  14.6 us (4%)
  between operations  13.8 us (4%)
  other arithmetic  12.8 us (4%)
    all_gather x3, waiting for transfers between devices, on_device(): back_rows = lax.all_gather(w_back[layer_id], 'sp', axis=1, tiled=True)  67.5 us
    all_gather x3, waiting for transfers between devices, on_device(): lax.all_gather(w_gate[layer_id], 'sp', axis=0, tiled=True)  65.1 us
    ppermute x9, waiting for transfers between devices, on_device(): lax.ppermute(ring[-1], 'tp', [(dev, (dev + 1) % 4) for dev in range(4)])  51.2 us
    all_gather x3, blocking collectives, on_device(): full_pooled = lax.all_gather(pooled, 'tp', axis=1, tiled=True)  48.7 us
    all_gather x3, waiting for transfers between devices, on_device(): lax.all_gather(w_pool_in[layer_id], 'sp', axis=0, tiled=True)  17.2 us
    all_to_all x3, starting transfers between devices, on_device(): lax.all_to_all(back_rows, 'tp', split_axis=1, concat_axis=0, tiled=True)  10.8 us
    ppermute x3, starting transfers between devices, padded_2(): before = lax.ppermute(last, axis, up)  10.1 us
    reduce_sum x3, other arithmetic, on_device(): jnp.mean(wide * wide, axis=-1, keepdims=True) + norm_eps  8.56 us
  transfers between devices with their start and end apart: 27, of which 18 were waited for; matrix products, arithmetic and copies ran while one was open for 11% of the time, Pallas kernels for 0%

profile of v1, /device:TPU:0, one launch (start us, length us, event | category | flops | bytes accessed | tf_op | source)
XLA Modules:
  0.0 332.4 jit_solution(5592557218177108179)
XLA Ops:
  6.5 2.1 fusion.192
  8.8 0.8 copy.33
  9.8 1.2 fusion.190
  11.6 0.8 copy.34
  13.8 5.2 %collective-permute-done = bf16[256,512]{1,0:T(8,128)(2,1)S(1)} collective-permute-done((bf16[256,512]{1,0:T(8,128)(2,1)S(1)}, bf16[256,512]{1,0:T(8,128)(2,1)S(1)}, u32[]{:S(2)}, u32[]{:S(2)}) %collective-permute-start) | collective-permute-done | bytes 262176 | tf_op jit(solution)/shard_map/ppermute | solution.py:66
  19.1 5.7 %collective-permute-done.1 = bf16[256,512]{1,0:T(8,128)(2,1)S(1)} collective-permute-done((bf16[256,512]{1,0:T(8,128)(2,1)S(1)}, bf16[256,512]{1,0:T(8,128)(2,1)S(1)}, u32[]{:S(2)}, u32[]{:S(2)}) %collective-permute-start.1) | collective-permute-done | bytes 262176 | tf_op jit(solution)/shard_map/ppermute | solution.py:66
  25.0 5.7 %collective-permute-done.2 = bf16[256,512]{1,0:T(8,128)(2,1)S(1)} collective-permute-done((bf16[256,512]{1,0:T(8,128)(2,1)S(1)}, bf16[256,512]{1,0:T(8,128)(2,1)S(1)}, u32[]{:S(2)}, u32[]{:S(2)}) %collective-permute-start.2) | collective-permute-done | bytes 262176 | tf_op jit(solution)/shard_map/ppermute | solution.py:66
  30.6 2.8 fusion
  33.5 6.1 %all-gather.21.cloned.1.call-done = bf16[1,2048,256]{2,1,0:T(8,128)(2,1)} async-done(((bf16[1,512,256]{2,1,0:T(8,128)(2,1)}), bf16[1,2048,256]{2,1,0:T(8,128)(2,1)}) %all-gather.21.cloned.1.call-update) | async-done | bytes 1048592 | tf_op jit(solution)/shard_map/all_gather | solution.py:80
  39.6 1.7 convolution_convert_fusion.5
  41.4 3.4 %collective-permute-start.3 = (bf16[8,32,256]{2,1,0:T(8,128)(2,1)S(1)}, bf16[8,32,256]{2,1,0:T(8,128)(2,1)S(1)}, u32[]{:S(2)}, u32[]{:S(2)}) collective-permute-start(bf16[8,32,256]{2,1,0:T(8,128)(2,1)S(1)} %bitcast.103), channel_id=1, source_target_pairs={{0,4},{4,8},{8,12},{1,5},{5,9},{9,13},{2,6},{6,10},{10,14},{3,7},{... | collective-permute-start | bytes 393224 | tf_op jit(solution)/shard_map/ppermute | solution.py:21
  44.7 1.3 collective-permute-start.4
  46.1 22.7 %all-gather.23.cloned.1.call-done = bf16[1,256,2048]{1,2,0:T(8,128)(2,1)} async-done(((bf16[1,256,512]{1,2,0:T(8,128)(2,1)}), bf16[1,256,2048]{1,2,0:T(8,128)(2,1)}) %all-gather.23.cloned.1.call-update) | async-done | bytes 1048592 | tf_op jit(solution)/shard_map/all_gather | solution.py:105
  68.8 2.3 copy.20
  71.1 3.5 %all-to-all-start = ((bf16[256,4,512]{2,0,1:T(8,128)(2,1)}), bf16[256,4,512]{2,0,1:T(8,128)(2,1)S(1)}, u32[]{:S(2)}, u32[]{:S(2)}) async-start(bf16[256,4,512]{2,0,1:T(8,128)(2,1)} %copy.20), calls=%async_computation | async-start | bytes 2097152 | tf_op jit(solution)/shard_map/all_to_all | solution.py:106
  75.3 0.8 fusion.172
  76.1 16.6 %all_gather.38 = bf16[256,1024]{1,0:T(8,128)(2,1)S(1)} all-gather(bf16[256,256]{1,0:T(8,128)(2,1)S(1)} %bitcast.112), channel_id=1, replica_groups=mesh['grp'=2,'sp'=4,'tp'=4] {'tp'}, dimensions={1}, use_global_device_ids=true | all-gather | bytes 655360 | tf_op jit(solution)/shard_map/all_gather | solution.py:104
  93.4 21.8 %all-gather.19.cloned.1.call-done = bf16[1,2048,512]{2,1,0:T(8,128)(2,1)} async-done(((bf16[1,512,512]{2,1,0:T(8,128)(2,1)}), bf16[1,2048,512]{2,1,0:T(8,128)(2,1)}) %all-gather.19.cloned.1.call-update) | async-done | bytes 2097168 | tf_op jit(solution)/shard_map/all_gather | solution.py:85
  115.2 2.4 fusion.75
  117.9 5.7 %collective-permute-done.5 = bf16[256,512]{1,0:T(8,128)(2,1)S(1)} collective-permute-done((bf16[256,512]{1,0:T(8,128)(2,1)S(1)}, bf16[256,512]{1,0:T(8,128)(2,1)S(1)}, u32[]{:S(2)}, u32[]{:S(2)}) %collective-permute-start.5) | collective-permute-done | bytes 262176 | tf_op jit(solution)/shard_map/ppermute | solution.py:66
  123.6 5.8 %collective-permute-done.6 = bf16[256,512]{1,0:T(8,128)(2,1)S(1)} collective-permute-done((bf16[256,512]{1,0:T(8,128)(2,1)S(1)}, bf16[256,512]{1,0:T(8,128)(2,1)S(1)}, u32[]{:S(2)}, u32[]{:S(2)}) %collective-permute-start.6) | collective-permute-done | bytes 262176 | tf_op jit(solution)/shard_map/ppermute | solution.py:66
  129.4 5.8 %collective-permute-done.7 = bf16[256,512]{1,0:T(8,128)(2,1)S(1)} collective-permute-done((bf16[256,512]{1,0:T(8,128)(2,1)S(1)}, bf16[256,512]{1,0:T(8,128)(2,1)S(1)}, u32[]{:S(2)}, u32[]{:S(2)}) %collective-permute-start.7) | collective-permute-done | bytes 262176 | tf_op jit(solution)/shard_map/ppermute | solution.py:66
  135.2 2.9 fusion.3
  138.0 5.4 %all-gather.27.cloned.1.call-done = bf16[1,2048,256]{2,1,0:T(8,128)(2,1)} async-done(((bf16[1,512,256]{2,1,0:T(8,128)(2,1)}), bf16[1,2048,256]{2,1,0:T(8,128)(2,1)}) %all-gather.27.cloned.1.call-update) | async-done | bytes 1048592 | tf_op jit(solution)/shard_map/all_gather | solution.py:80
  143.5 1.7 convolution_convert_fusion.4
  145.2 3.4 %collective-permute-start.8 = (bf16[8,32,256]{2,1,0:T(8,128)(2,1)S(1)}, bf16[8,32,256]{2,1,0:T(8,128)(2,1)S(1)}, u32[]{:S(2)}, u32[]{:S(2)}) collective-permute-start(bf16[8,32,256]{2,1,0:T(8,128)(2,1)S(1)} %bitcast.99), channel_id=1, source_target_pairs={{0,4},{4,8},{8,12},{1,5},{5,9},{9,13},{2,6},{6,10},{10,14},{3,7},{... | collective-permute-start | bytes 393224 | tf_op jit(solution)/shard_map/ppermute | solution.py:21
  148.6 1.3 collective-permute-start.9
  149.9 0.8 copy.35
  150.7 22.1 %all-gather.29.cloned.1.call-done = bf16[1,256,2048]{1,2,0:T(8,128)(2,1)} async-done(((bf16[1,256,512]{1,2,0:T(8,128)(2,1)}), bf16[1,256,2048]{1,2,0:T(8,128)(2,1)}) %all-gather.29.cloned.1.call-update) | async-done | bytes 1048592 | tf_op jit(solution)/shard_map/all_gather | solution.py:105
  172.8 2.3 copy.24
  175.1 3.5 %all-to-all-start.1 = ((bf16[256,4,512]{2,0,1:T(8,128)(2,1)}), bf16[256,4,512]{2,0,1:T(8,128)(2,1)S(1)}, u32[]{:S(2)}, u32[]{:S(2)}) async-start(bf16[256,4,512]{2,0,1:T(8,128)(2,1)} %copy.24), calls=%async_computation.1 | async-start | bytes 2097152 | tf_op jit(solution)/shard_map/all_to_all | solution.py:106
  180.6 16.1 %all_gather.42 = bf16[256,1024]{1,0:T(8,128)(2,1)S(1)} all-gather(bf16[256,256]{1,0:T(8,128)(2,1)S(1)} %bitcast.113), channel_id=1, replica_groups=mesh['grp'=2,'sp'=4,'tp'=4] {'tp'}, dimensions={1}, use_global_device_ids=true | all-gather | bytes 655360 | tf_op jit(solution)/shard_map/all_gather | solution.py:104
  197.4 21.4 %all-gather.25.cloned.1.call-done = bf16[1,2048,512]{2,1,0:T(8,128)(2,1)} async-done(((bf16[1,512,512]{2,1,0:T(8,128)(2,1)}), bf16[1,2048,512]{2,1,0:T(8,128)(2,1)}) %all-gather.25.cloned.1.call-update) | async-done | bytes 2097168 | tf_op jit(solution)/shard_map/all_gather | solution.py:85
  218.8 2.4 fusion.72
  221.3 5.8 %collective-permute-done.10 = bf16[256,512]{1,0:T(8,128)(2,1)S(1)} collective-permute-done((bf16[256,512]{1,0:T(8,128)(2,1)S(1)}, bf16[256,512]{1,0:T(8,128)(2,1)S(1)}, u32[]{:S(2)}, u32[]{:S(2)}) %collective-permute-start.10) | collective-permute-done | bytes 262176 | tf_op jit(solution)/shard_map/ppermute | solution.py:66
  227.1 5.8 %collective-permute-done.11 = bf16[256,512]{1,0:T(8,128)(2,1)S(1)} collective-permute-done((bf16[256,512]{1,0:T(8,128)(2,1)S(1)}, bf16[256,512]{1,0:T(8,128)(2,1)S(1)}, u32[]{:S(2)}, u32[]{:S(2)}) %collective-permute-start.11) | collective-permute-done | bytes 262176 | tf_op jit(solution)/shard_map/ppermute | solution.py:66
  232.9 5.8 %collective-permute-done.12 = bf16[256,512]{1,0:T(8,128)(2,1)S(1)} collective-permute-done((bf16[256,512]{1,0:T(8,128)(2,1)S(1)}, bf16[256,512]{1,0:T(8,128)(2,1)S(1)}, u32[]{:S(2)}, u32[]{:S(2)}) %collective-permute-start.12) | collective-permute-done | bytes 262176 | tf_op jit(solution)/shard_map/ppermute | solution.py:66
  238.7 2.9 fusion.6
  241.6 5.6 %all-gather.33.cloned.1.call-done = bf16[1,2048,256]{2,1,0:T(8,128)(2,1)} async-done(((bf16[1,512,256]{2,1,0:T(8,128)(2,1)}), bf16[1,2048,256]{2,1,0:T(8,128)(2,1)}) %all-gather.33.cloned.1.call-update) | async-done | bytes 1048592 | tf_op jit(solution)/shard_map/all_gather | solution.py:80
  247.2 1.7 convolution_convert_fusion.3
  248.9 3.4 %collective-permute-start.13 = (bf16[8,32,256]{2,1,0:T(8,128)(2,1)S(1)}, bf16[8,32,256]{2,1,0:T(8,128)(2,1)S(1)}, u32[]{:S(2)}, u32[]{:S(2)}) collective-permute-start(bf16[8,32,256]{2,1,0:T(8,128)(2,1)S(1)} %bitcast.107), channel_id=1, source_target_pairs={{0,4},{4,8},{8,12},{1,5},{5,9},{9,13},{2,6},{6,10},{10,14},{3,7},{... | collective-permute-start | bytes 393224 | tf_op jit(solution)/shard_map/ppermute | solution.py:21
  252.3 1.3 collective-permute-start.14
  253.6 22.8 %all-gather.35.cloned.1.call-done = bf16[1,256,2048]{1,2,0:T(8,128)(2,1)} async-done(((bf16[1,256,512]{1,2,0:T(8,128)(2,1)}), bf16[1,256,2048]{1,2,0:T(8,128)(2,1)}) %all-gather.35.cloned.1.call-update) | async-done | bytes 1048592 | tf_op jit(solution)/shard_map/all_gather | solution.py:105
  276.3 2.3 copy.28
  278.6 3.7 %all-to-all-start.2 = ((bf16[256,4,512]{2,0,1:T(8,128)(2,1)}), bf16[256,4,512]{2,0,1:T(8,128)(2,1)S(1)}, u32[]{:S(2)}, u32[]{:S(2)}) async-start(bf16[256,4,512]{2,0,1:T(8,128)(2,1)} %copy.28), calls=%async_computation.2 | async-start | bytes 2097152 | tf_op jit(solution)/shard_map/all_to_all | solution.py:106
  284.3 16.0 %all_gather.46 = bf16[256,1024]{1,0:T(8,128)(2,1)S(1)} all-gather(bf16[256,256]{1,0:T(8,128)(2,1)S(1)} %bitcast.111), channel_id=1, replica_groups=mesh['grp'=2,'sp'=4,'tp'=4] {'tp'}, dimensions={1}, use_global_device_ids=true | all-gather | bytes 655360 | tf_op jit(solution)/shard_map/all_gather | solution.py:104
  300.9 21.9 %all-gather.31.cloned.1.call-done = bf16[1,2048,512]{2,1,0:T(8,128)(2,1)} async-done(((bf16[1,512,512]{2,1,0:T(8,128)(2,1)}), bf16[1,2048,512]{2,1,0:T(8,128)(2,1)}) %all-gather.31.cloned.1.call-update) | async-done | bytes 2097168 | tf_op jit(solution)/shard_map/all_gather | solution.py:85
  322.8 3.1 fusion.69
  (118 shorter events, 8.9 us)
Async XLA Ops:
  6.5 2.2 copy-start.1
  6.5 3.2 copy-start
  6.5 33.1 %all-gather.21.cloned.1.call-start = ((), (), s32[]{:S(2)}) async-start(), calls=%async_computation.4 | async-start | bytes 1310720 | tf_op jit(solution)/shard_map/all_gather | solution.py:80
  8.7 60.1 %all-gather.23.cloned.1.call-start = ((), (), s32[]{:S(2)}) async-start(), calls=%async_computation.5 | async-start | bytes 1310720 | tf_op jit(solution)/shard_map/all_gather | solution.py:105
  9.7 2.8 copy-start.2
  9.7 3.4 %copy-start.5 = (f32[3,2048]{1,0:T(4,128)S(1)}, f32[3,2048]{1,0:T(4,128)}, u32[]{:S(2)}) copy-start(f32[3,2048]{1,0:T(4,128)} %param.8) | copy-start | bytes 73732
  9.7 105.5 %all-gather.19.cloned.1.call-start = ((), (), s32[]{:S(2)}) async-start(), calls=%async_computation.3 | async-start | bytes 2621440 | tf_op jit(solution)/shard_map/all_gather | solution.py:85
  11.0 132.5 %all-gather.27.cloned.1.call-start = ((), (), s32[]{:S(2)}) async-start(), calls=%async_computation.7 | async-start | bytes 1310720 | tf_op jit(solution)/shard_map/all_gather | solution.py:80
  11.6 161.2 %all-gather.29.cloned.1.call-start = ((), (), s32[]{:S(2)}) async-start(), calls=%async_computation.8 | async-start | bytes 1310720 | tf_op jit(solution)/shard_map/all_gather | solution.py:105
  12.5 206.3 %all-gather.25.cloned.1.call-start = ((), (), s32[]{:S(2)}) async-start(), calls=%async_computation.6 | async-start | bytes 2621440 | tf_op jit(solution)/shard_map/all_gather | solution.py:85
  12.5 6.5 %collective-permute-start = (bf16[256,512]{1,0:T(8,128)(2,1)S(1)}, bf16[256,512]{1,0:T(8,128)(2,1)S(1)}, u32[]{:S(2)}, u32[]{:S(2)}) collective-permute-start(bf16[256,512]{1,0:T(8,128)(2,1)S(1)} %copy-done.2), channel_id=1, source_target_pairs={{0,1},{1,2},{2,3},{3,0},{4,5},{5,6},{6,7},{7,4},{8,9},{9,10},{10,1... | collective-permute-start | bytes 786440 | tf_op jit(solution)/shard_map/ppermute | solution.py:66
  13.7 57.4 %copy-start.9 = (f32[1,2048]{1,0:T(1,128)}, f32[1,2048]{1,0:T(1,128)S(1)}, u32[]{:S(2)}) copy-start(f32[1,2048]{1,0:T(1,128)S(1)} %get-tuple-element.34) | copy-start | bytes 24580
  19.0 5.8 %collective-permute-start.1 = (bf16[256,512]{1,0:T(8,128)(2,1)S(1)}, bf16[256,512]{1,0:T(8,128)(2,1)S(1)}, u32[]{:S(2)}, u32[]{:S(2)}) collective-permute-start(bf16[256,512]{1,0:T(8,128)(2,1)S(1)} %collective-permute-done), channel_id=1, source_target_pairs={{0,1},{1,2},{2,3},{3,0},{4,5},{5,6},{6,7},{7,4},{8,9},{9,10},{10,1... | collective-permute-start | bytes 786440 | tf_op jit(solution)/shard_map/ppermute | solution.py:66
  24.8 5.8 %collective-permute-start.2 = (bf16[256,512]{1,0:T(8,128)(2,1)S(1)}, bf16[256,512]{1,0:T(8,128)(2,1)S(1)}, u32[]{:S(2)}, u32[]{:S(2)}) collective-permute-start(bf16[256,512]{1,0:T(8,128)(2,1)S(1)} %collective-permute-done.1), channel_id=1, source_target_pairs={{0,1},{1,2},{2,3},{3,0},{4,5},{5,6},{6,7},{7,4},{8,9},{9,10},{10,1... | collective-permute-start | bytes 786440 | tf_op jit(solution)/shard_map/ppermute | solution.py:66
  33.5 37.6 %copy-start.24 = (f32[256]{0:T(256)}, f32[256]{0:T(256)S(1)}, u32[]{:S(2)}) copy-start(f32[256]{0:T(256)S(1)} %add_rsqrt_fusion.2) | copy-start | bytes 3076
  41.4 33.4 %collective-permute-start.3 = (bf16[8,32,256]{2,1,0:T(8,128)(2,1)S(1)}, bf16[8,32,256]{2,1,0:T(8,128)(2,1)S(1)}, u32[]{:S(2)}, u32[]{:S(2)}) collective-permute-start(bf16[8,32,256]{2,1,0:T(8,128)(2,1)S(1)} %bitcast.103), channel_id=1, source_target_pairs={{0,4},{4,8},{8,12},{1,5},{5,9},{9,13},{2,6},{6,10},{10,14},{3,7},{... | collective-permute-start | bytes 393224 | tf_op jit(solution)/shard_map/ppermute | solution.py:21
  44.7 30.0 %collective-permute-start.4 = (bf16[8,32,256]{2,1,0:T(8,128)(2,1)S(1)}, bf16[8,32,256]{2,1,0:T(8,128)(2,1)S(1)}, u32[]{:S(2)}, u32[]{:S(2)}) collective-permute-start(bf16[8,32,256]{2,1,0:T(8,128)(2,1)S(1)} %bitcast.104), channel_id=1, source_target_pairs={{4,0},{8,4},{12,8},{5,1},{9,5},{13,9},{6,2},{10,6},{14,10},{7,3},{... | collective-permute-start | bytes 393224 | tf_op jit(solution)/shard_map/ppermute | solution.py:22
  46.1 29.2 %copy-start.10 = (pred[256]{0:T(512)(128)(4,1)}, pred[256]{0:T(512)(128)(4,1)S(1)}, u32[]{:S(2)}) copy-start(pred[256]{0:T(512)(128)(4,1)S(1)} %get-tuple-element.44) | copy-start | bytes 772
  46.1 29.2 %copy-start.13 = (pred[256]{0:T(512)(128)(4,1)}, pred[256]{0:T(512)(128)(4,1)S(1)}, u32[]{:S(2)}) copy-start(pred[256]{0:T(512)(128)(4,1)S(1)} %get-tuple-element.45) | copy-start | bytes 772
  46.1 29.1 %copy-start.16 = (pred[256]{0:T(512)(128)(4,1)}, pred[256]{0:T(512)(128)(4,1)S(1)}, u32[]{:S(2)}) copy-start(pred[256]{0:T(512)(128)(4,1)S(1)} %get-tuple-element.46) | copy-start | bytes 772
  46.1 29.1 %copy-start.19 = (pred[256]{0:T(512)(128)(4,1)}, pred[256]{0:T(512)(128)(4,1)S(1)}, u32[]{:S(2)}) copy-start(pred[256]{0:T(512)(128)(4,1)S(1)} %get-tuple-element.47) | copy-start | bytes 772
  71.1 21.8 %all-to-all-start = ((bf16[256,4,512]{2,0,1:T(8,128)(2,1)}), bf16[256,4,512]{2,0,1:T(8,128)(2,1)S(1)}, u32[]{:S(2)}, u32[]{:S(2)}) async-start(bf16[256,4,512]{2,0,1:T(8,128)(2,1)} %copy.20), calls=%async_computation | async-start | bytes 2097152 | tf_op jit(solution)/shard_map/all_to_all | solution.py:106
  74.7 172.5 %all-gather.33.cloned.1.call-start = ((), (), s32[]{:S(2)}) async-start(), calls=%async_computation.10 | async-start | bytes 1310720 | tf_op jit(solution)/shard_map/all_gather | solution.py:80
  117.7 25.8 %copy-start.3 = (bf16[256,512]{1,0:T(8,128)(2,1)}, bf16[256,512]{1,0:T(8,128)(2,1)S(1)}, u32[]{:S(2)}) copy-start(bf16[256,512]{1,0:T(8,128)(2,1)S(1)} %fusion.75) | copy-start | bytes 786436
  117.7 25.8 %copy-start.7 = (f32[1,2048]{1,0:T(1,128)S(1)}, f32[1,2048]{1,0:T(1,128)}, u32[]{:S(2)}) copy-start(f32[1,2048]{1,0:T(1,128)} %get-tuple-element.35) | copy-start | bytes 24580
  117.7 5.8 %collective-permute-start.5 = (bf16[256,512]{1,0:T(8,128)(2,1)S(1)}, bf16[256,512]{1,0:T(8,128)(2,1)S(1)}, u32[]{:S(2)}, u32[]{:S(2)}) collective-permute-start(bf16[256,512]{1,0:T(8,128)(2,1)S(1)} %fusion.75), channel_id=1, source_target_pairs={{0,1},{1,2},{2,3},{3,0},{4,5},{5,6},{6,7},{7,4},{8,9},{9,10},{10,1... | collective-permute-start | bytes 786440 | tf_op jit(solution)/shard_map/ppermute | solution.py:66
  117.8 158.5 %all-gather.35.cloned.1.call-start = ((), (), s32[]{:S(2)}) async-start(), calls=%async_computation.11 | async-start | bytes 1310720 | tf_op jit(solution)/shard_map/all_gather | solution.py:105
  123.6 5.8 %collective-permute-start.6 = (bf16[256,512]{1,0:T(8,128)(2,1)S(1)}, bf16[256,512]{1,0:T(8,128)(2,1)S(1)}, u32[]{:S(2)}, u32[]{:S(2)}) collective-permute-start(bf16[256,512]{1,0:T(8,128)(2,1)S(1)} %collective-permute-done.5), channel_id=1, source_target_pairs={{0,1},{1,2},{2,3},{3,0},{4,5},{5,6},{6,7},{7,4},{8,9},{9,10},{10,1... | collective-permute-start | bytes 786440 | tf_op jit(solution)/shard_map/ppermute | solution.py:66
  129.4 5.8 %collective-permute-start.7 = (bf16[256,512]{1,0:T(8,128)(2,1)S(1)}, bf16[256,512]{1,0:T(8,128)(2,1)S(1)}, u32[]{:S(2)}, u32[]{:S(2)}) collective-permute-start(bf16[256,512]{1,0:T(8,128)(2,1)S(1)} %collective-permute-done.6), channel_id=1, source_target_pairs={{0,1},{1,2},{2,3},{3,0},{4,5},{5,6},{6,7},{7,4},{8,9},{9,10},{10,1... | collective-permute-start | bytes 786440 | tf_op jit(solution)/shard_map/ppermute | solution.py:66
  138.0 37.0 %copy-start.22 = (f32[256]{0:T(256)}, f32[256]{0:T(256)S(1)}, u32[]{:S(2)}) copy-start(f32[256]{0:T(256)S(1)} %add_rsqrt_fusion.1) | copy-start | bytes 3076
  145.2 33.4 %collective-permute-start.8 = (bf16[8,32,256]{2,1,0:T(8,128)(2,1)S(1)}, bf16[8,32,256]{2,1,0:T(8,128)(2,1)S(1)}, u32[]{:S(2)}, u32[]{:S(2)}) collective-permute-start(bf16[8,32,256]{2,1,0:T(8,128)(2,1)S(1)} %bitcast.99), channel_id=1, source_target_pairs={{0,4},{4,8},{8,12},{1,5},{5,9},{9,13},{2,6},{6,10},{10,14},{3,7},{... | collective-permute-start | bytes 393224 | tf_op jit(solution)/shard_map/ppermute | solution.py:21
  148.6 30.1 %collective-permute-start.9 = (bf16[8,32,256]{2,1,0:T(8,128)(2,1)S(1)}, bf16[8,32,256]{2,1,0:T(8,128)(2,1)S(1)}, u32[]{:S(2)}, u32[]{:S(2)}) collective-permute-start(bf16[8,32,256]{2,1,0:T(8,128)(2,1)S(1)} %bitcast.100), channel_id=1, source_target_pairs={{4,0},{8,4},{12,8},{5,1},{9,5},{13,9},{6,2},{10,6},{14,10},{7,3},{... | collective-permute-start | bytes 393224 | tf_op jit(solution)/shard_map/ppermute | solution.py:22
  175.1 21.8 %all-to-all-start.1 = ((bf16[256,4,512]{2,0,1:T(8,128)(2,1)}), bf16[256,4,512]{2,0,1:T(8,128)(2,1)S(1)}, u32[]{:S(2)}, u32[]{:S(2)}) async-start(bf16[256,4,512]{2,0,1:T(8,128)(2,1)} %copy.24), calls=%async_computation.1 | async-start | bytes 2097152 | tf_op jit(solution)/shard_map/all_to_all | solution.py:106
  178.6 144.2 %all-gather.31.cloned.1.call-start = ((), (), s32[]{:S(2)}) async-start(), calls=%async_computation.9 | async-start | bytes 2621440 | tf_op jit(solution)/shard_map/all_gather | solution.py:85
  179.0 0.7 copy-start.11
  179.1 0.7 copy-start.20
  180.5 38.2 %copy-start.8 = (f32[1,2048]{1,0:T(1,128)S(1)}, f32[1,2048]{1,0:T(1,128)}, u32[]{:S(2)}) copy-start(f32[1,2048]{1,0:T(1,128)} %get-tuple-element.35) | copy-start | bytes 24580
  180.6 38.2 %copy-start.23 = (f32[256]{0:T(256)S(1)}, f32[256]{0:T(256)}, u32[]{:S(2)}) copy-start(f32[256]{0:T(256)} %copy-done.22) | copy-start | bytes 3076
  221.2 25.9 %copy-start.4 = (bf16[256,512]{1,0:T(8,128)(2,1)}, bf16[256,512]{1,0:T(8,128)(2,1)S(1)}, u32[]{:S(2)}) copy-start(bf16[256,512]{1,0:T(8,128)(2,1)S(1)} %fusion.72) | copy-start | bytes 786436
  221.2 25.9 %copy-start.6 = (f32[1,2048]{1,0:T(1,128)S(1)}, f32[1,2048]{1,0:T(1,128)}, u32[]{:S(2)}) copy-start(f32[1,2048]{1,0:T(1,128)} %get-tuple-element.33) | copy-start | bytes 24580
  221.2 5.8 %collective-permute-start.10 = (bf16[256,512]{1,0:T(8,128)(2,1)S(1)}, bf16[256,512]{1,0:T(8,128)(2,1)S(1)}, u32[]{:S(2)}, u32[]{:S(2)}) collective-permute-start(bf16[256,512]{1,0:T(8,128)(2,1)S(1)} %fusion.72), channel_id=1, source_target_pairs={{0,1},{1,2},{2,3},{3,0},{4,5},{5,6},{6,7},{7,4},{8,9},{9,10},{10,1... | collective-permute-start | bytes 786440 | tf_op jit(solution)/shard_map/ppermute | solution.py:66
  227.1 5.8 %collective-permute-start.11 = (bf16[256,512]{1,0:T(8,128)(2,1)S(1)}, bf16[256,512]{1,0:T(8,128)(2,1)S(1)}, u32[]{:S(2)}, u32[]{:S(2)}) collective-permute-start(bf16[256,512]{1,0:T(8,128)(2,1)S(1)} %collective-permute-done.10), channel_id=1, source_target_pairs={{0,1},{1,2},{2,3},{3,0},{4,5},{5,6},{6,7},{7,4},{8,9},{9,10},{10,1... | collective-permute-start | bytes 786440 | tf_op jit(solution)/shard_map/ppermute | solution.py:66
  232.9 5.8 %collective-permute-start.12 = (bf16[256,512]{1,0:T(8,128)(2,1)S(1)}, bf16[256,512]{1,0:T(8,128)(2,1)S(1)}, u32[]{:S(2)}, u32[]{:S(2)}) collective-permute-start(bf16[256,512]{1,0:T(8,128)(2,1)S(1)} %collective-permute-done.11), channel_id=1, source_target_pairs={{0,1},{1,2},{2,3},{3,0},{4,5},{5,6},{6,7},{7,4},{8,9},{9,10},{10,1... | collective-permute-start | bytes 786440 | tf_op jit(solution)/shard_map/ppermute | solution.py:66
  248.9 33.5 %collective-permute-start.13 = (bf16[8,32,256]{2,1,0:T(8,128)(2,1)S(1)}, bf16[8,32,256]{2,1,0:T(8,128)(2,1)S(1)}, u32[]{:S(2)}, u32[]{:S(2)}) collective-permute-start(bf16[8,32,256]{2,1,0:T(8,128)(2,1)S(1)} %bitcast.107), channel_id=1, source_target_pairs={{0,4},{4,8},{8,12},{1,5},{5,9},{9,13},{2,6},{6,10},{10,14},{3,7},{... | collective-permute-start | bytes 393224 | tf_op jit(solution)/shard_map/ppermute | solution.py:21
  252.3 30.1 %collective-permute-start.14 = (bf16[8,32,256]{2,1,0:T(8,128)(2,1)S(1)}, bf16[8,32,256]{2,1,0:T(8,128)(2,1)S(1)}, u32[]{:S(2)}, u32[]{:S(2)}) collective-permute-start(bf16[8,32,256]{2,1,0:T(8,128)(2,1)S(1)} %bitcast.108), channel_id=1, source_target_pairs={{4,0},{8,4},{12,8},{5,1},{9,5},{13,9},{6,2},{10,6},{14,10},{7,3},{... | collective-permute-start | bytes 393224 | tf_op jit(solution)/shard_map/ppermute | solution.py:22
  278.6 21.8 %all-to-all-start.2 = ((bf16[256,4,512]{2,0,1:T(8,128)(2,1)}), bf16[256,4,512]{2,0,1:T(8,128)(2,1)S(1)}, u32[]{:S(2)}, u32[]{:S(2)}) async-start(bf16[256,4,512]{2,0,1:T(8,128)(2,1)} %copy.28), calls=%async_computation.2 | async-start | bytes 2097152 | tf_op jit(solution)/shard_map/all_to_all | solution.py:106
  282.7 0.7 copy-start.12
  282.8 0.7 copy-start.21
  (4 other events, 2.6 us)
Sparse Core Ops, SparseCore 0:
  8.9 30.6 all-gather.20
  41.2 27.5 all-gather.22
  70.4 44.8 all-gather.18
  116.7 26.7 all-gather.26
  144.9 27.8 all-gather.28
  174.2 44.5 all-gather.24
  220.4 26.7 all-gather.32
  248.7 27.5 all-gather.34
  277.9 44.8 all-gather.30
